TPU v7x, 32 devices: a whole 2x2x4 slice. The times are simulated.
32 devices in a mesh: sp: 4 (over y, x), tp: 8 (over z, core).
Axes of the slice: x: 2, y: 2, z: 4, core: 2. Of those that a mesh axis runs over, the one named last changes fastest.
Arguments:
- tokens: bfloat16 [3, 2048, 4096], P(None, 'sp', 'tp'), may hold values from -6 to 6
- new_token: bfloat16 [3, 1, 4096], P(None, None, 'tp'), may hold values from -6 to 6
- query_weight: bfloat16 [4096, 4096], P(None, 'tp'), may hold values from -0.09375 to 0.09375
- key_weight: bfloat16 [4096, 4096], P(None, 'tp'), may hold values from -0.09375 to 0.09375
- value_weight: bfloat16 [4096, 4096], P(None, 'tp'), may hold values from -0.09375 to 0.09375
- log_decay: float32 [64], P('tp'), may hold values from -0.034 to 0
Outputs:
- state: bfloat16 [3, 64, 64, 64], P(None, 'tp', 'sp')
- read: bfloat16 [3, 4096], P(None, 'tp')
All inputs are finite; a program needn't handle non-finite values.
Results may differ from a plain program's by a relative error of at most 0.012.
Values may be sent and summed in bfloat16 or wider, within the bound.
A program may use at most 64 MiB of HBM per device.

v0:
```python
import jax
import jax.numpy as jnp
from jax import lax
from jax.sharding import PartitionSpec as P

HD = 64


def rotate(values, positions):
    half_dim = values.shape[-1] // 2
    inverse = 10000.0 ** (-jnp.arange(half_dim, dtype=jnp.float32) / half_dim)
    angles = positions.astype(jnp.float32)[:, None, None] * inverse[None, None, :]
    cosine = jnp.cos(angles)
    sine_part = jnp.sin(angles)
    first = values[..., :half_dim]
    second = values[..., half_dim:]
    return jnp.concatenate(
        [first * cosine - second * sine_part, first * sine_part + second * cosine], axis=-1
    )


def group_norm(output):
    centered = output - jnp.mean(output, axis=-1, keepdims=True)
    return centered * lax.rsqrt(jnp.mean(centered * centered, axis=-1, keepdims=True) + 1e-05)


def body(tokens, new_token, query_weight, key_weight, value_weight, log_decay):
    sequences, span_len, _ = tokens.shape
    head_count = log_decay.shape[0]
    inner = head_count * HD
    groups = lax.axis_size("sp")
    own_index = lax.axis_index("sp")
    key_scale = HD ** (-0.5)
    key_share = HD // groups
    row_weights = jnp.concatenate([key_weight, value_weight], axis=1)
    all_weights = jnp.concatenate([key_weight, value_weight, query_weight], axis=1)
    row_piece = lax.all_gather(tokens, "tp", axis=2, tiled=True)
    new_piece = lax.all_gather(new_token, "tp", axis=2, tiled=True)
    row_total = jnp.dot(row_piece, row_weights, preferred_element_type=jnp.float32)
    new_total = jnp.dot(new_piece, all_weights, preferred_element_type=jnp.float32)
    row_total = row_total.reshape(sequences, span_len, 2, head_count, HD)
    offsets = own_index * span_len + jnp.arange(span_len, dtype=jnp.int32)
    key_rows = (rotate(row_total[:, :, 0], offsets) * key_scale).astype(jnp.bfloat16)
    value_rows = row_total[:, :, 1].astype(jnp.bfloat16)
    to_end = (span_len - 1 - jnp.arange(span_len, dtype=jnp.int32)).astype(jnp.float32)
    decay_rows = jnp.exp(to_end[:, None] * log_decay[None, :])
    weighted = (key_rows.astype(jnp.float32) * decay_rows[None, :, :, None]).astype(jnp.bfloat16)
    span_state = jnp.einsum(
        "sthk,sthv->shkv", weighted, value_rows, preferred_element_type=jnp.float32
    )
    carried_state = jnp.exp(log_decay * (span_len * (groups - 1 - own_index)).astype(jnp.float32))
    scaled_state = span_state * carried_state[None, :, None, None]
    state_rows = lax.psum_scatter(scaled_state, "sp", scatter_dimension=2, tiled=True)
    new_total = new_total.reshape(sequences, 1, 3, head_count, HD)
    new_position = jnp.full((1,), groups * span_len, jnp.int32)
    fresh_key = (rotate(new_total[:, :, 0], new_position) * key_scale).astype(jnp.bfloat16)[:, 0]
    new_value = new_total[:, 0, 1].astype(jnp.bfloat16)
    new_query = rotate(new_total[:, :, 2], new_position).astype(jnp.bfloat16)[:, 0]
    query_entries = new_query.astype(jnp.float32)
    decay_one = jnp.exp(log_decay)[None, :, None]
    query_share = lax.dynamic_slice_in_dim(query_entries, own_index * key_share, key_share, 2)
    partial_read = (
        jnp.einsum("shkv,shk->shv", state_rows, query_share, precision=lax.Precision.HIGHEST)
        * decay_one
    )
    summed = lax.psum(partial_read, "sp")
    own_term = jnp.sum(
        query_entries * fresh_key.astype(jnp.float32), axis=-1, keepdims=True
    ) * new_value.astype(jnp.float32)
    normed = group_norm(summed + own_term)
    return (state_rows.astype(jnp.bfloat16), normed.reshape(sequences, inner).astype(jnp.bfloat16))


def solution(mesh):
    return jax.shard_map(
        body,
        mesh=mesh,
        in_specs=(
            P(None, "sp", "tp"),
            P(None, None, "tp"),
            P(None, "tp"),
            P(None, "tp"),
            P(None, "tp"),
            P("tp"),
        ),
        out_specs=(P(None, "tp", "sp", None), P(None, "tp")),
        check_vma=False,
    )
```

profile of v0, /device:TPU:0, one launch (start us, length us, event | category | flops | bytes accessed | tf_op | source)
XLA Modules:
  0.0 200.9 jit_solution(10623617118696532471)
XLA Ops:
  7.2 0.0 all-gather.2.cloned.1.call-start
  7.2 0.7 all-gather.2.cloned.1.call-update
  7.9 0.0 reduce-scatter.2.cloned.1.call-start
  7.9 6.4 %copy.9 = bf16[4096,512]{0,1:T(8,128)(2,1)} copy(bf16[4096,512]{1,0:T(8,128)(2,1)} %param.10) | data formatting | bytes 8388608 | tf_op args[4]
  14.3 0.0 copy-start
  14.3 0.0 copy-start.1
  14.3 6.5 %copy.8 = bf16[4096,512]{0,1:T(8,128)(2,1)} copy(bf16[4096,512]{1,0:T(8,128)(2,1)} %param.9) | data formatting | bytes 8388608 | tf_op args[3]
  20.8 0.0 copy-done
  20.8 16.8 %all_gather.7 = bf16[3,1,4096]{2,0,1:T(4,128)(2,1)S(1)} all-gather(bf16[3,1,512]{2,0,1:T(4,128)(2,1)S(1)} %copy-done), channel_id=1, replica_groups=mesh['sp'=4,'tp'=8] {'tp'}, dimensions={2}, use_global_device_ids=true | all-gather | bytes 27648 | tf_op jit(solution)/shard_map/all_gather | solution.py:38
  37.7 0.0 copy-done.1
  37.7 0.1 multiply_exponential_fusion
  37.8 0.3 multiply_cosine_fusion
  38.1 91.1 %all-gather.2.cloned.1.call-done = bf16[3,512,4096]{2,1,0:T(8,128)(2,1)} async-done(((bf16[3,512,512]{2,1,0:T(8,128)(2,1)}), bf16[3,512,4096]{2,1,0:T(8,128)(2,1)}) %all-gather.2.cloned.1.call-update) | async-done | bytes 12582928 | tf_op jit(solution)/shard_map/all_gather | solution.py:37
  129.3 18.5 %fusion.7 = f32[1024,3,512]{2,0,1:T(8,128)S(1)} fusion(bf16[3,512,4096]{2,1,0:T(8,128)(2,1)} %all-gather.2.cloned.1.call-done, bf16[4096,512]{0,1:T(8,128)(2,1)} %copy.9, bf16[4096,512]{0,1:T(8,128)(2,1)} %copy.8), kind=kOutput, calls=%fused_computation.8 | convolution fusion | flops 12901679104 | bytes 27262976 | tf_op jit(solution)/shard_map/dot_general | solution.py:39
  147.8 0.3 copy_bitcast_fusion
  148.1 0.5 multiply_subtract_fusion
  148.5 1.5 fusion.20
  150.0 0.0 reduce-scatter.2.cloned.1.call-update
  150.0 5.6 %fusion.11 = f32[3,1536]{1,0:T(4,128)S(1)} fusion(bf16[4096,512]{1,0:T(8,128)(2,1)} %param.8, bf16[4096,512]{1,0:T(8,128)(2,1)} %param.10, bf16[4096,512]{1,0:T(8,128)(2,1)} %param.9, bf16[3,1,4096]{2,0,1:T(4,128)(2,1)S(1)} %all_gather.7), kind=kOutput, calls=%fused_computation.16 | convolution fusion | flops 75497472 | bytes 12625920 | tf_op jit(solution)/shard_map/dot_general | solution.py:40
  155.6 0.1 reshape.216
  155.7 0.1 multiply_sine_fusion.1
  155.8 0.1 subtract_bitcast_fusion
  155.8 0.1 fusion.31
  155.9 18.7 %reduce-scatter.2.cloned.1.call-done = f32[3,8,16,64]{3,2,1,0:T(8,128)} async-done(((f32[3,8,64,64]{3,2,1,0:T(8,128)}), f32[3,8,16,64]{3,2,1,0:T(8,128)}) %reduce-scatter.2.cloned.1.call-update) | async-done | bytes 98320 | tf_op jit(solution)/shard_map/reduce_scatter | solution.py:53
  174.6 1.1 fusion.27
  175.7 0.1 broadcast_multiply_fusion
  175.8 15.0 %psum.7 = f32[3,8,64]{2,1,0:T(8,128)S(1)} all-reduce(f32[3,8,64]{2,1,0:T(8,128)S(1)} %broadcast_multiply_fusion), channel_id=1, replica_groups=mesh['sp'=4,'tp'=8] {'sp'}, use_global_device_ids=true, to_apply=%region_1.0 | all-reduce | flops 1536 | bytes 12288 | tf_op jit(solution)/shard_map/psum | solution.py:66
  190.8 0.7 fusion.38
  191.6 0.2 multiply_reduce_fusion
  191.7 0.1 multiply_convert_fusion.4
  191.8 0.7 convert_element_type.83
  192.5 1.6 convert_element_type.76
  (7 shorter events, 0.0 us)
Async XLA Ops:
  7.2 122.1 %all-gather.2.cloned.1.call-start = ((), (), s32[]{:S(2)}) async-start(), calls=%async_computation.1 | async-start | bytes 14155776 | tf_op jit(solution)/shard_map/all_gather | solution.py:37
  7.9 166.7 %reduce-scatter.2.cloned.1.call-start = ((), (), s32[]{:S(2)}) async-start(), calls=%async_computation.2 | async-start | bytes 983040 | tf_op jit(solution)/shard_map/reduce_scatter | solution.py:53
  14.3 6.5 %copy-start = (bf16[3,1,512]{2,0,1:T(4,128)(2,1)S(1)}, bf16[3,1,512]{2,0,1:T(4,128)(2,1)}, u32[]{:S(2)}) copy-start(bf16[3,1,512]{2,0,1:T(4,128)(2,1)} %param.7) | copy-start | bytes 9220
  14.3 23.4 %copy-start.1 = (f32[8]{0:T(128)S(1)}, f32[8]{0:T(128)}, u32[]{:S(2)}) copy-start(f32[8]{0:T(128)} %param.11) | copy-start | bytes 100
Sparse Core Ops, SparseCore 0:
  9.6 119.6 all-gather.1
  150.1 24.4 reduce-scatter.1
where the time goes:
time: 201 us
  waiting for transfers between devices  110 us (55%)
  blocking collectives  31.9 us (16%)
  matrix products  26.7 us (13%)
  between operations  14.1 us (7%)
  local copies, waits for them, and re-layouts  14 us (7%)
  other arithmetic  3.69 us (2%)
    all_gather x1, waiting for transfers between devices, body(): row_piece = lax.all_gather(tokens, 'tp', axis=2, tiled=True)  91.1 us
    reduce_scatter x1, waiting for transfers between devices, body(): lax.psum_scatter(scaled_state, 'sp', scatter_dimension=2, tiled=True)  18.7 us
    dot_general x1, matrix products, body(): jnp.dot(row_piece, row_weights, preferred_element_type=jnp.float32)  18.5 us
    all_gather x1, blocking collectives, body(): new_piece = lax.all_gather(new_token, 'tp', axis=2, tiled=True)  16.8 us
    psum x1, blocking collectives, body(): summed = lax.psum(partial_read, 'sp')  15 us
    unnamed x6, local copies, waits for them, and re-layouts  12.9 us
    dot_general x1, matrix products, body(): jnp.dot(new_piece, all_weights, preferred_element_type=jnp.float32)  5.59 us
  transfers between devices with their start and end apart: 2, of which 2 were waited for; matrix products, arithmetic and copies ran while one was open for 10% of the time, Pallas kernels for 0%

commit v1 on v0

--- a/solution.py
+++ b/solution.py
@@ -63,7 +63,8 @@
         jnp.einsum("shkv,shk->shv", state_rows, query_share, precision=lax.Precision.HIGHEST)
         * decay_one
     )
-    summed = lax.psum(partial_read, "sp")
+    parts = lax.all_gather(partial_read, "sp", axis=0, tiled=False)
+    summed = parts.sum(axis=0)
     own_term = jnp.sum(
         query_entries * fresh_key.astype(jnp.float32), axis=-1, keepdims=True
     ) * new_value.astype(jnp.float32)

time: 201 us -> 194 us (0.965)
  blocking collectives: 31.9 us -> 25.1 us
    psum x1 -> x0, blocking collectives: 15 us -> none  [body(): summed = lax.psum(partial_read, 'sp')]
    all_gather x0 -> x1, blocking collectives: none -> 8.26 us  [body(): parts = lax.all_gather(partial_read, 'sp', axis=0, tiled=False)]
    all_gather x1, waiting for transfers between devices: 91.1 us -> 85.3 us  [body(): row_piece = lax.all_gather(tokens, 'tp', axis=2, tiled=True)]
    reduce_scatter x1, waiting for transfers between devices: 18.7 us -> 23.9 us  [body(): lax.psum_scatter(scaled_state, 'sp', scatter_dimension=2, tiled=True)]
where the time goes in v1:
time: 194 us
  waiting for transfers between devices  110 us (57%)
  matrix products  26.8 us (14%)
  blocking collectives  25.1 us (13%)
  between operations  14.1 us (7%)
  local copies, waits for them, and re-layouts  13.9 us (7%)
  other arithmetic  3.86 us (2%)
    all_gather x1, waiting for transfers between devices, body(): row_piece = lax.all_gather(tokens, 'tp', axis=2, tiled=True)  85.3 us
    reduce_scatter x1, waiting for transfers between devices, body(): lax.psum_scatter(scaled_state, 'sp', scatter_dimension=2, tiled=True)  23.9 us
    dot_general x1, matrix products, body(): jnp.dot(row_piece, row_weights, preferred_element_type=jnp.float32)  18.5 us
    all_gather x1, blocking collectives, body(): new_piece = lax.all_gather(new_token, 'tp', axis=2, tiled=True)  16.8 us
    unnamed x6, local copies, waits for them, and re-layouts  12.9 us
    all_gather x1, blocking collectives, body(): parts = lax.all_gather(partial_read, 'sp', axis=0, tiled=False)  8.26 us
    dot_general x1, matrix products, body(): jnp.dot(new_piece, all_weights, preferred_element_type=jnp.float32)  5.7 us
  transfers between devices with their start and end apart: 2, of which 2 were waited for; matrix products, arithmetic and copies ran while one was open for 10% of the time, Pallas kernels for 0%

profile of v1, /device:TPU:0, one launch (start us, length us, event | category | flops | bytes accessed | tf_op | source)
XLA Modules:
  0.0 193.8 jit_solution(7615783362770031967)
XLA Ops:
  7.2 0.0 all-gather.3.cloned.1.call-start
  7.2 0.7 all-gather.3.cloned.1.call-update
  7.9 0.0 reduce-scatter.2.cloned.1.call-start
  7.9 6.4 %copy.14 = bf16[4096,512]{0,1:T(8,128)(2,1)} copy(bf16[4096,512]{1,0:T(8,128)(2,1)} %param.10) | data formatting | bytes 8388608 | tf_op args[4]
  14.4 0.0 copy-start
  14.4 6.5 %copy.13 = bf16[4096,512]{0,1:T(8,128)(2,1)} copy(bf16[4096,512]{1,0:T(8,128)(2,1)} %param.9) | data formatting | bytes 8388608 | tf_op args[3]
  20.9 0.0 copy-done
  20.9 16.8 %all_gather.13 = bf16[3,1,4096]{2,0,1:T(4,128)(2,1)S(1)} all-gather(bf16[3,1,512]{2,0,1:T(4,128)(2,1)S(1)} %copy-done), channel_id=1, replica_groups=mesh['sp'=4,'tp'=8] {'tp'}, dimensions={2}, use_global_device_ids=true | all-gather | bytes 27648 | tf_op jit(solution)/shard_map/all_gather | solution.py:38
  37.7 0.0 copy-start.1
  37.7 5.7 %fusion.10 = f32[3,1536]{1,0:T(4,128)S(1)} fusion(bf16[4096,512]{1,0:T(8,128)(2,1)} %param.8, bf16[4096,512]{1,0:T(8,128)(2,1)} %param.10, bf16[4096,512]{1,0:T(8,128)(2,1)} %param.9, bf16[3,1,4096]{2,0,1:T(4,128)(2,1)S(1)} %all_gather.13), kind=kOutput, calls=%fused_computation.15 | convolution fusion | flops 75497472 | bytes 12625920 | tf_op jit(solution)/shard_map/dot_general | solution.py:40
  43.4 0.1 reshape.223
  43.5 0.1 multiply_sine_fusion.1
  43.6 0.0 copy-done.1
  43.6 0.1 multiply_exponential_fusion
  43.7 0.3 multiply_cosine_fusion
  44.0 85.3 %all-gather.3.cloned.1.call-done = bf16[3,512,4096]{2,1,0:T(8,128)(2,1)} async-done(((bf16[3,512,512]{2,1,0:T(8,128)(2,1)}), bf16[3,512,4096]{2,1,0:T(8,128)(2,1)}) %all-gather.3.cloned.1.call-update) | async-done | bytes 12582928 | tf_op jit(solution)/shard_map/all_gather | solution.py:37
  129.3 18.5 %fusion.6 = f32[1024,3,512]{2,0,1:T(8,128)S(1)} fusion(bf16[3,512,4096]{2,1,0:T(8,128)(2,1)} %all-gather.3.cloned.1.call-done, bf16[4096,512]{0,1:T(8,128)(2,1)} %copy.14, bf16[4096,512]{0,1:T(8,128)(2,1)} %copy.13), kind=kOutput, calls=%fused_computation.7 | convolution fusion | flops 12901679104 | bytes 27262976 | tf_op jit(solution)/shard_map/dot_general | solution.py:39
  147.8 0.3 copy_bitcast_fusion
  148.1 0.5 multiply_subtract_fusion
  148.5 1.5 fusion.19
  150.0 0.0 reduce-scatter.2.cloned.1.call-update
  150.0 0.1 subtract_bitcast_fusion
  150.1 0.2 multiply_reduce_fusion.1
  150.3 0.1 mul.283
  150.3 0.1 mul.284
  150.4 0.1 reshape.224
  150.5 0.1 fusion.28
  150.6 23.9 %reduce-scatter.2.cloned.1.call-done = f32[3,8,16,64]{3,2,1,0:T(8,128)} async-done(((f32[3,8,64,64]{3,2,1,0:T(8,128)}), f32[3,8,16,64]{3,2,1,0:T(8,128)}) %reduce-scatter.2.cloned.1.call-update) | async-done | bytes 98320 | tf_op jit(solution)/shard_map/reduce_scatter | solution.py:53
  174.5 1.1 fusion.25
  175.7 0.1 broadcast_multiply_fusion
  175.7 8.3 %all-gather = f32[12,8,64]{2,1,0:T(8,128)S(1)} all-gather(f32[3,8,64]{2,1,0:T(8,128)S(1)} %broadcast_multiply_fusion), channel_id=2, replica_groups=mesh['sp'=4,'tp'=8] {'sp'}, dimensions={0}, use_global_device_ids=true | all-gather | bytes 30720 | tf_op jit(solution)/shard_map/all_gather | solution.py:66
  184.0 0.2 fusion.29
  184.2 0.1 reduce_sum.39
  184.2 0.2 multiply_reduce_fusion
  184.4 0.1 mul.288
  184.5 0.1 mul.289
  184.6 0.1 sub.41
  184.6 0.1 sub.42
  184.7 0.6 multiply_convert_fusion.4
  185.3 1.6 convert_element_type.83
  (9 shorter events, 0.1 us)
Async XLA Ops:
  7.2 122.1 %all-gather.3.cloned.1.call-start = ((), (), s32[]{:S(2)}) async-start(), calls=%async_computation.1 | async-start | bytes 14155776 | tf_op jit(solution)/shard_map/all_gather | solution.py:37
  7.9 166.6 %reduce-scatter.2.cloned.1.call-start = ((), (), s32[]{:S(2)}) async-start(), calls=%async_computation.2 | async-start | bytes 983040 | tf_op jit(solution)/shard_map/reduce_scatter | solution.py:53
  14.4 6.5 %copy-start = (bf16[3,1,512]{2,0,1:T(4,128)(2,1)S(1)}, bf16[3,1,512]{2,0,1:T(4,128)(2,1)}, u32[]{:S(2)}) copy-start(bf16[3,1,512]{2,0,1:T(4,128)(2,1)} %param.7) | copy-start | bytes 9220
  37.7 5.9 %copy-start.1 = (f32[8]{0:T(128)S(1)}, f32[8]{0:T(128)}, u32[]{:S(2)}) copy-start(f32[8]{0:T(128)} %param.11) | copy-start | bytes 100
Sparse Core Ops, SparseCore 0:
  9.6 119.6 all-gather.2
  150.1 24.3 reduce-scatter.1
